TPU v7x, 512 devices: a whole 4x4x16 slice. The times are simulated.
512 devices in a mesh: kv: 32 (over z, core), tp: 16 (over y, x).
Axes of the slice: x: 4, y: 4, z: 16, core: 2. Of those that a mesh axis runs over, the one named last changes fastest.
Arguments:
- tokens: bfloat16 [16, 2048], P(None, 'kv'), may hold values from -8 to 8
- lengths: int32 [16], replicated, may hold values from 1 to 49152, 196608 in all
- latent_cache: bfloat16 [16, 49152, 256], P(None, ('kv', 'tp')), may hold values from -10 to 10
- rope_cache: bfloat16 [16, 49152, 32], P(None, ('kv', 'tp')), may hold values from -2000 to 2000
- gain_in: bfloat16 [2048], P('kv'), may hold values from 0.099609375 to 1.8984375
- w_down_q: bfloat16 [2048, 512], P('kv'), may hold values from -0.125 to 0.125
- w_down_kv: bfloat16 [2048, 256], P('kv'), may hold values from -0.125 to 0.125
- w_rope_key: bfloat16 [2048, 32], P('kv'), may hold values from -0.125 to 0.125
- gain_q: bfloat16 [512], replicated, may hold values from 0.099609375 to 1.8984375
- w_up_qn: bfloat16 [512, 16, 64], replicated, may hold values from -0.25 to 0.25
- w_up_qr: bfloat16 [512, 16, 32], replicated, may hold values from -0.25 to 0.25
- gain_kv: bfloat16 [256], replicated, may hold values from 0.099609375 to 1.8984375
- w_key_up: bfloat16 [256, 16, 64], replicated, may hold values from -0.375 to 0.375
- w_value_up: bfloat16 [256, 16, 64], replicated, may hold values from -0.375 to 0.375
- w_attn_out: bfloat16 [16, 64, 2048], P('tp', None, 'kv'), may hold values from -0.1875 to 0.1875
- gain_mid: bfloat16 [2048], P('kv'), may hold values from 0.099609375 to 1.8984375
- w_ff_in: bfloat16 [2048, 8192], P('kv', 'tp'), may hold values from -0.125 to 0.125
- w_ff_out: bfloat16 [8192, 2048], P('tp', 'kv'), may hold values from -0.0625 to 0.0625
Outputs:
- mixed: bfloat16 [16, 2048], P(None, 'kv')
- new_latent: bfloat16 [16, 256], replicated
- new_rope_key: bfloat16 [16, 32], replicated
Inputs may be any that keep to these rules, and one draw needn't show every extreme that they name: `lengths`: each sequence's live cache positions; one sequence fills the whole cache.
All inputs are finite; a program needn't handle non-finite values.
Results may differ from a plain program's by a relative error of at most 0.012.
Values sent between devices are 32-bit elements; how exact they have to be, the bound alone decides.
A program may use at most 64 MiB of HBM per device.

v0:
```python
import jax
import jax.numpy as jnp
from jax import lax
from jax.sharding import Mesh
from jax.sharding import PartitionSpec as P

D = 2048
NOPE = 64
ROPE = 32
KV = ("kv_0", "kv_1")
KV_TP = ("kv_0", "kv_1", "tp_0", "tp_1")
TP = ("tp_0", "tp_1")
EPS = 1e-06


def over_axes(value, axes):
    for axis in axes:
        value = lax.psum(value, axis)
    return value


def copy_for_each(value, axis):
    size = lax.axis_size(axis)
    return lax.all_to_all(
        jnp.broadcast_to(value[None], (size, *value.shape)), axis, 0, 0, tiled=True
    )


def gathered_once(value, axis):
    leaves = jax.tree.leaves(value)
    order = sorted(range(len(leaves)), key=lambda k: -leaves[k].size)
    width = (1, *leaves[order[0]].shape)[-1]
    lines = [
        jnp.pad(leaves[k].reshape(-1), (0, -leaves[k].size % width)).reshape(-1, width)
        for k in order
    ]
    both, at, found = (copy_for_each(jnp.concatenate(lines), axis), 0, {})
    for k, line in zip(order, lines):
        piece = both[:, at : at + len(line)].reshape(len(both), -1)
        found[k] = piece[:, : leaves[k].size].reshape(-1, *leaves[k].shape)
        at += len(line)
    numbers = iter(range(len(leaves)))
    return jax.tree.map(lambda _: found[next(numbers)], value)


def joined_by_halves(pieces, combine):
    while len(jax.tree.leaves(pieces)[0]) > 1:
        pieces = jax.vmap(combine)(
            *(jax.tree.map(lambda part: part[side::2], pieces) for side in (0, 1))
        )
    return jax.tree.map(lambda part: part[0], pieces)


def joined_all(value, axis, combine):
    pieces = gathered_once(value, axis)
    return joined_by_halves(pieces, combine)


def of_everyone(value, axis):
    everything = copy_for_each(value, axis)
    return jnp.sum(everything, axis=0)


def in_one(arrays, axis):
    ravelled, at, outs = (jnp.concatenate([a.reshape(-1) for a in arrays]), 0, [])
    subtotal = of_everyone(ravelled, axis)
    for a in arrays:
        outs.append(subtotal[at : at + a.size].reshape(a.shape))
        at += a.size
    return tuple(outs)


def rotate(values, positions):
    half = values.shape[-1] // 2
    inverse = 10000.0 ** (-jnp.arange(half, dtype=jnp.float32) / half)
    angle = positions.astype(jnp.float32)[:, None, None] * inverse[None, None, :]
    first = values[..., :half]
    second = values[..., half:]
    return jnp.concatenate(
        [
            first * jnp.cos(angle) - second * jnp.sin(angle),
            second * jnp.cos(angle) + first * jnp.sin(angle),
        ],
        axis=-1,
    )


def rms_scaled(values, gain):
    return (
        values
        * lax.rsqrt(jnp.mean(values * values, axis=-1, keepdims=True) + EPS)
        * gain.astype(jnp.float32)
    )


def combine(earlier, later):
    top_a, total_a, acc_a = earlier
    top_b, total_b, acc_b = later
    top = jnp.maximum(top_a, top_b)
    fade_a = jnp.exp(top_a - top)
    fade_b = jnp.exp(top_b - top)
    return (
        top,
        total_a * fade_a + total_b * fade_b,
        acc_a * fade_a[..., None] + acc_b * fade_b[..., None],
    )


def fold_sources(parts):
    tops, totals, accs = parts
    top = jnp.max(tops, axis=0)
    fade = jnp.exp(tops - top[None])
    return (top, jnp.sum(totals * fade, axis=0), jnp.sum(accs * fade[..., None], axis=0))


def per_device(
    tokens,
    lengths,
    latent_cache,
    rope_cache,
    gain_in,
    w_down_q,
    w_down_kv,
    w_rope_key,
    gain_q,
    w_up_qn,
    w_up_qr,
    gain_kv,
    w_key_up,
    w_value_up,
    w_attn_out,
    gain_mid,
    w_ff_in,
    w_ff_out,
):
    f32 = jnp.float32
    bf16 = jnp.bfloat16
    scale = (NOPE + ROPE) ** (-0.5)
    resid = tokens.astype(f32)
    scaled_in = (resid * gain_in.astype(f32)).astype(bf16)
    part_q = jnp.dot(scaled_in, w_down_q, preferred_element_type=f32)
    part_kv = jnp.dot(scaled_in, w_down_kv, preferred_element_type=f32)
    part_rope = jnp.dot(scaled_in, w_rope_key, preferred_element_type=f32)
    square_in = jnp.sum(resid * resid, axis=1)
    sum_q, sum_kv, sum_rope, total_in = (
        over_axes(part_q, KV),
        over_axes(part_kv, KV),
        over_axes(part_rope, KV),
        over_axes(square_in, KV),
    )
    inv_in = lax.rsqrt(total_in / D + EPS)[:, None]
    query_latent = rms_scaled(inv_in * sum_q, gain_q).astype(bf16)
    new_latent = rms_scaled(inv_in * sum_kv, gain_kv).astype(bf16)
    new_rope_key = rotate((inv_in * sum_rope)[:, None, :], lengths)[:, 0, :].astype(bf16)
    query_nope = jnp.einsum(
        "bc,chd->bhd", query_latent, w_up_qn, preferred_element_type=f32
    ).astype(bf16)
    query_rope = rotate(
        jnp.einsum("bc,chr->bhr", query_latent, w_up_qr, preferred_element_type=f32), lengths
    ).astype(bf16)
    query_cache = jnp.einsum(
        "bhd,khd->bhk", query_nope, w_key_up, preferred_element_type=f32
    ).astype(bf16)
    rows = latent_cache.shape[1]
    positions = lax.axis_index(KV_TP) * rows + jnp.arange(rows, dtype=jnp.int32)
    live = (positions[None, :] < lengths[:, None])[:, None, :]
    scores = (
        jnp.einsum("bhk,blk->bhl", query_cache, latent_cache, preferred_element_type=f32)
        + jnp.einsum("bhr,blr->bhl", query_rope, rope_cache, preferred_element_type=f32)
    ) * scale
    scores = jnp.where(live, scores, -1e30)
    top = jnp.max(scores, axis=2)
    weights = jnp.where(live, jnp.exp(scores - top[:, :, None]), 0.0)
    total = jnp.sum(weights, axis=2)
    acc = jnp.einsum("bhl,blk->bhk", weights.astype(bf16), latent_cache, preferred_element_type=f32)
    heads_dev = w_attn_out.shape[0]
    first_head = lax.axis_index(TP) * heads_dev
    own_value_up = lax.dynamic_slice_in_dim(w_value_up, first_head, heads_dev, 1).astype(f32)
    own_cache_q = lax.dynamic_slice_in_dim(query_cache, first_head, heads_dev, 1)
    own_rope_q = lax.dynamic_slice_in_dim(query_rope, first_head, heads_dev, 1)
    self_score = (
        jnp.einsum("bhk,bk->bh", own_cache_q, new_latent, preferred_element_type=f32)
        + jnp.einsum("bhr,br->bh", own_rope_q, new_rope_key, preferred_element_type=f32)
    ) * scale
    expanded = jnp.einsum("bhk,khv->bhv", acc, w_value_up.astype(f32))
    top, total, expanded = fold_sources(
        (
            lax.all_to_all(top[None], TP, split_axis=2, concat_axis=0, tiled=True),
            lax.all_to_all(total[None], TP, split_axis=2, concat_axis=0, tiled=True),
            lax.all_to_all(expanded[None], TP, split_axis=2, concat_axis=0, tiled=True),
        )
    )
    top, total, expanded = joined_all((top, total, expanded), KV, combine)
    joined = jnp.maximum(top, self_score)
    fade = jnp.exp(top - joined)
    self_weight = jnp.exp(self_score - joined)
    total = total * fade + self_weight
    self_value = jnp.einsum("bk,khv->bhv", new_latent.astype(f32), own_value_up)
    expanded = (
        expanded * fade[:, :, None] + self_weight.astype(bf16).astype(f32)[:, :, None] * self_value
    )
    head_out = (expanded / total[:, :, None]).astype(bf16)
    attn_part = jnp.einsum("bhv,hvd->bd", head_out, w_attn_out, preferred_element_type=f32)
    resid_mid = resid + over_axes(attn_part, TP)
    scaled_mid = (resid_mid * gain_mid.astype(f32)).astype(bf16)
    hidden_part = jnp.dot(scaled_mid, w_ff_in, preferred_element_type=f32)
    square_mid = jnp.sum(resid_mid * resid_mid, axis=1)
    hidden_sum, total_mid = in_one((hidden_part, square_mid), KV)
    inv_mid = lax.rsqrt(total_mid / D + EPS)[:, None]
    hidden = jnp.square(jax.nn.relu(inv_mid * hidden_sum)).astype(bf16)
    out_part = jnp.dot(hidden, w_ff_out, preferred_element_type=f32)
    mixed = (resid_mid + over_axes(out_part, TP)).astype(bf16)
    return (mixed, new_latent, new_rope_key)


def solution(mesh):
    finer = Mesh(mesh.devices.reshape(16, 2, 4, 4), ("kv_0", "kv_1", "tp_0", "tp_1"))
    in_specs = (
        P(None, KV),
        P(),
        P(None, KV_TP, None),
        P(None, KV_TP, None),
        P(KV),
        P(KV, None),
        P(KV, None),
        P(KV, None),
        P(),
        P(),
        P(),
        P(),
        P(),
        P(),
        P(TP, None, KV),
        P(KV),
        P(KV, TP),
        P(TP, KV),
    )
    out_specs = (P(None, KV), P(), P())
    return jax.shard_map(
        per_device, mesh=finer, in_specs=in_specs, out_specs=out_specs, check_vma=False
    )
```

profile of v0, /device:TPU:2, one launch (start us, length us, event | category | flops | bytes accessed | tf_op | source)
XLA Modules:
  0.0 240.8 jit_solution(12234813138934605315)
XLA Ops:
  0.7 0.8 convert_element_type.73
  1.5 0.7 convert_element_type.80
  2.1 0.8 fusion.36
  2.9 0.7 broadcast_compare_fusion
  3.7 0.7 convert_element_type.75
  4.3 0.8 fusion.55
  5.2 0.9 fusion.57
  6.1 1.0 fusion.59
  7.1 62.1 %all-reduce.2 = (f32[16,256]{1,0:T(8,128)S(1)}, f32[16]{0:T(128)S(1)}, f32[16,512]{1,0:T(8,128)S(1)}, f32[16,32]{1,0:T(8,128)S(1)}) all-reduce(f32[16,256]{1,0:T(8,128)S(1)} %fusion.57, f32[16]{0:T(128)S(1)} %fusion.36, f32[16,512]{1,0:T(8,128)S(1)} %fusion.59, ...), channel_id=1, replica_groups=mesh['kv_0'=16,'kv_1'=2,'tp_0'=4,'tp_1'=4] {'kv_0'}, use_global_device_ids=true, to_apply=%region_11.12 | all-reduce | flops 12816 | bytes 102528 | tf_op jit(solution)/shard_map/psum | solution.py:18
  69.2 3.6 %all-reduce.3 = (f32[16,256]{1,0:T(8,128)S(1)}, f32[16]{0:T(128)S(1)}, f32[16,512]{1,0:T(8,128)S(1)}, f32[16,32]{1,0:T(8,128)S(1)}) all-reduce(f32[16,256]{1,0:T(8,128)S(1)} %get-tuple-element.3, f32[16]{0:T(128)S(1)} %get-tuple-element.4, ...), channel_id=1, replica_groups=mesh['kv_0'=16,'kv_1'=2,'tp_0'=4,'tp_1'=4] {'kv_1'}, use_global_device_ids=true, to_apply=%region_12.13 | all-reduce | flops 12816 | bytes 102528 | tf_op jit(solution)/shard_map/psum | solution.py:18
  72.8 0.2 multiply_reduce_fusion
  73.1 1.5 fusion.78
  74.7 0.7 convolution_convert_fusion
  75.5 0.1 fusion.13
  75.7 0.1 copy-done.1
  75.8 0.4 fusion.85
  76.2 0.7 copy.58
  76.9 7.5 %all-to-all-start.1 = ((f32[1,16,16]{1,0,2:T(1,128)}), f32[1,16,16]{1,0,2:T(1,128)S(1)}, u32[]{:S(2)}, u32[]{:S(2)}) async-start(f32[1,16,16]{1,0,2:T(1,128)} %copy.58), calls=%async_computation.1 | async-start | bytes 16384 | tf_op jit(solution)/shard_map/all_to_all | solution.py:188
  84.6 0.3 fusion.11
  84.9 0.2 fusion.86
  85.1 0.2 fusion.9
  85.3 0.7 reshape.385
  86.1 0.7 copy.59
  86.8 3.8 %all-to-all-done.1 = f32[1,16,16]{1,0,2:T(1,128)S(1)} async-done(((f32[1,16,16]{1,0,2:T(1,128)}), f32[1,16,16]{1,0,2:T(1,128)S(1)}, u32[]{:S(2)}, u32[]{:S(2)}) %all-to-all-start.1) | async-done | bytes 1056 | tf_op jit(solution)/shard_map/all_to_all | solution.py:188
  90.5 4.7 %all-to-all-start.2 = ((f32[1,16,16]{1,0,2:T(1,128)}), f32[1,16,16]{1,0,2:T(1,128)S(1)}, u32[]{:S(2)}, u32[]{:S(2)}) async-start(f32[1,16,16]{1,0,2:T(1,128)} %copy.59), calls=%async_computation.2 | async-start | bytes 16384 | tf_op jit(solution)/shard_map/all_to_all | solution.py:189
  95.3 6.2 %all-to-all-done.2 = f32[1,16,16]{1,0,2:T(1,128)S(1)} async-done(((f32[1,16,16]{1,0,2:T(1,128)}), f32[1,16,16]{1,0,2:T(1,128)S(1)}, u32[]{:S(2)}, u32[]{:S(2)}) %all-to-all-start.2) | async-done | bytes 1056 | tf_op jit(solution)/shard_map/all_to_all | solution.py:189
  101.5 4.6 %all-to-all-start = ((f32[16,1,1024]{2,1,0:T(1,128)}), f32[16,1,1024]{2,1,0:T(1,128)S(1)}, u32[]{:S(2)}, u32[]{:S(2)}) async-start(f32[16,1,1024]{2,1,0:T(1,128)} %reshape.385), calls=%async_computation | async-start | bytes 131072 | tf_op jit(solution)/shard_map/all_to_all | solution.py:190
  106.1 6.3 %all-to-all-done = f32[16,1,1024]{2,1,0:T(1,128)S(1)} async-done(((f32[16,1,1024]{2,1,0:T(1,128)}), f32[16,1,1024]{2,1,0:T(1,128)S(1)}, u32[]{:S(2)}, u32[]{:S(2)}) %all-to-all-start) | async-done | bytes 65568 | tf_op jit(solution)/shard_map/all_to_all | solution.py:190
  112.5 0.5 broadcast.232
  113.0 0.8 reduce.11
  114.0 0.8 reshape.387
  114.9 7.0 %all-to-all-start.3 = ((f32[32,1,1152]{2,1,0:T(1,128)}), f32[32,1,1152]{2,1,0:T(1,128)S(1)}, u32[]{:S(2)}, u32[]{:S(2)}) async-start(f32[32,1,1152]{2,1,0:T(1,128)} %reshape.387), calls=%async_computation.3 | async-start | bytes 294912 | tf_op jit(solution)/shard_map/all_to_all | solution.py:24
  121.9 0.8 fusion.45
  122.7 0.2 multiply_reduce_fusion.1
  122.9 0.2 fusion.25
  123.1 16.7 %all-to-all-done.3 = f32[32,1,1152]{2,1,0:T(1,128)S(1)} async-done(((f32[32,1,1152]{2,1,0:T(1,128)}), f32[32,1,1152]{2,1,0:T(1,128)S(1)}, u32[]{:S(2)}, u32[]{:S(2)}) %all-to-all-start.3) | async-done | bytes 147488 | tf_op jit(solution)/shard_map/all_to_all | solution.py:24
  139.8 1.0 reduce.12
  141.9 0.3 fusion.5
  142.1 8.9 %psum.92 = f32[16,64]{1,0:T(8,128)S(1)} all-reduce(f32[16,64]{1,0:T(8,128)S(1)} %fusion.5), channel_id=1, replica_groups=mesh['kv_0'=16,'kv_1'=2,'tp_0'=4,'tp_1'=4] {'tp_0'}, use_global_device_ids=true, to_apply=%region_16.17 | all-reduce | flops 1024 | bytes 8192 | tf_op jit(solution)/shard_map/psum | solution.py:18
  151.1 9.3 %psum.93 = f32[16,64]{1,0:T(8,128)S(1)} all-reduce(f32[16,64]{1,0:T(8,128)S(1)} %psum.92), channel_id=1, replica_groups=mesh['kv_0'=16,'kv_1'=2,'tp_0'=4,'tp_1'=4] {'tp_1'}, use_global_device_ids=true, to_apply=%region_17.18 | all-reduce | flops 1024 | bytes 8192 | tf_op jit(solution)/shard_map/psum | solution.py:18
  160.6 0.5 broadcast_in_dim.38
  161.2 60.2 %all_to_all.68 = f32[32,1,8208]{2,1,0:T(1,128)S(1)} all-to-all(f32[32,1,8208]{2,1,0:T(1,128)S(1)} %broadcast_in_dim.38), channel_id=1, replica_groups=mesh['kv_0'=16,'kv_1'=2,'tp_0'=4,'tp_1'=4] {'kv_0','kv_1'}, dimensions={0} | all-to-all | bytes 2101248 | tf_op jit(solution)/shard_map/all_to_all | solution.py:24
  221.4 0.6 reduce_sum.79
  222.1 0.2 copy-done.8
  222.2 0.2 fusion.23
  222.4 8.7 %psum.94 = f32[16,64]{1,0:T(8,128)S(1)} all-reduce(f32[16,64]{1,0:T(8,128)S(1)} %fusion.23), channel_id=1, replica_groups=mesh['kv_0'=16,'kv_1'=2,'tp_0'=4,'tp_1'=4] {'tp_0'}, use_global_device_ids=true, to_apply=%region_20.21 | all-reduce | flops 1024 | bytes 8192 | tf_op jit(solution)/shard_map/psum | solution.py:18
  231.2 9.0 %psum.95 = f32[16,64]{1,0:T(8,128)S(1)} all-reduce(f32[16,64]{1,0:T(8,128)S(1)} %psum.94), channel_id=1, replica_groups=mesh['kv_0'=16,'kv_1'=2,'tp_0'=4,'tp_1'=4] {'tp_1'}, use_global_device_ids=true, to_apply=%region_21.22 | all-reduce | flops 1024 | bytes 8192 | tf_op jit(solution)/shard_map/psum | solution.py:18
  240.2 0.6 add_convert_fusion.1
  (87 shorter events, 2.2 us)
Async XLA Ops:
  0.6 74.0 %copy-start = (bf16[512,16,64]{0,2,1:T(8,128)(2,1)S(1)}, bf16[512,16,64]{0,2,1:T(8,128)(2,1)}, u32[]{:S(2)}) copy-start(bf16[512,16,64]{0,2,1:T(8,128)(2,1)} %param.27) | copy-start | bytes 3145732
  0.6 74.0 %copy-start.3 = (bf16[256,16,64]{0,2,1:T(8,128)(2,1)S(1)}, bf16[256,16,64]{0,2,1:T(8,128)(2,1)}, u32[]{:S(2)}) copy-start(bf16[256,16,64]{0,2,1:T(8,128)(2,1)} %param.30) | copy-start | bytes 1572868
  74.6 0.9 copy-start.5
  74.6 1.2 copy-start.1
  75.8 9.0 %copy-start.2 = (bf16[256,16,64]{0,2,1:T(8,128)(2,1)S(1)}, bf16[256,16,64]{0,2,1:T(8,128)(2,1)}, u32[]{:S(2)}) copy-start(bf16[256,16,64]{0,2,1:T(8,128)(2,1)} %param.31) | copy-start | bytes 1572868
  76.9 13.6 %all-to-all-start.1 = ((f32[1,16,16]{1,0,2:T(1,128)}), f32[1,16,16]{1,0,2:T(1,128)S(1)}, u32[]{:S(2)}, u32[]{:S(2)}) async-start(f32[1,16,16]{1,0,2:T(1,128)} %copy.58), calls=%async_computation.1 | async-start | bytes 16384 | tf_op jit(solution)/shard_map/all_to_all | solution.py:188
  86.1 36.6 %copy-start.10 = (bf16[64]{0:T(256)(128)(2,1)S(1)}, bf16[64]{0:T(256)(128)(2,1)}, u32[]{:S(2)}) copy-start(bf16[64]{0:T(256)(128)(2,1)} %param.33) | copy-start | bytes 388
  86.1 36.6 %copy-start.11 = (bf16[256]{0:T(256)(128)(2,1)S(1)}, bf16[256]{0:T(256)(128)(2,1)}, u32[]{:S(2)}) copy-start(bf16[256]{0:T(256)(128)(2,1)} %param.29) | copy-start | bytes 1540
  90.5 11.0 %all-to-all-start.2 = ((f32[1,16,16]{1,0,2:T(1,128)}), f32[1,16,16]{1,0,2:T(1,128)S(1)}, u32[]{:S(2)}, u32[]{:S(2)}) async-start(f32[1,16,16]{1,0,2:T(1,128)} %copy.59), calls=%async_computation.2 | async-start | bytes 16384 | tf_op jit(solution)/shard_map/all_to_all | solution.py:189
  101.5 11.0 %all-to-all-start = ((f32[16,1,1024]{2,1,0:T(1,128)}), f32[16,1,1024]{2,1,0:T(1,128)S(1)}, u32[]{:S(2)}, u32[]{:S(2)}) async-start(f32[16,1,1024]{2,1,0:T(1,128)} %reshape.385), calls=%async_computation | async-start | bytes 131072 | tf_op jit(solution)/shard_map/all_to_all | solution.py:190
  114.9 24.9 %all-to-all-start.3 = ((f32[32,1,1152]{2,1,0:T(1,128)}), f32[32,1,1152]{2,1,0:T(1,128)S(1)}, u32[]{:S(2)}, u32[]{:S(2)}) async-start(f32[32,1,1152]{2,1,0:T(1,128)} %reshape.387), calls=%async_computation.3 | async-start | bytes 294912 | tf_op jit(solution)/shard_map/all_to_all | solution.py:24
  123.1 18.8 %copy-start.7 = (bf16[16,256]{1,0:T(8,128)(2,1)}, bf16[16,256]{1,0:T(8,128)(2,1)S(1)}, u32[]{:S(2)}) copy-start(bf16[16,256]{1,0:T(8,128)(2,1)S(1)} %get-tuple-element.28) | copy-start | bytes 24580
  140.7 1.1 copy-start.9
  140.9 19.5 %copy-start.4 = (bf16[16,64]{1,0:T(8,128)(2,1)S(1)}, bf16[16,64]{1,0:T(8,128)(2,1)}, u32[]{:S(2)}) copy-start(bf16[16,64]{1,0:T(8,128)(2,1)} %param.18) | copy-start | bytes 6148
  140.9 19.6 %copy-start.6 = (bf16[64,512]{1,0:T(8,128)(2,1)S(1)}, bf16[64,512]{1,0:T(8,128)(2,1)}, u32[]{:S(2)}) copy-start(bf16[64,512]{1,0:T(8,128)(2,1)} %param.34) | copy-start | bytes 196612
  221.4 0.8 copy-start.8
where the time goes:
time: 242 us; the launch traced here: 241 us
  blocking collectives  162 us (67%)
  waiting for transfers between devices  33 us (14%)
  starting transfers between devices  23.7 us (10%)
  other arithmetic  9.57 us (4%)
  matrix products  6.51 us (3%)
  local copies, waits for them, and re-layouts  5 us (2%)
    psum x6, blocking collectives, over_axes(): value = lax.psum(value, axis)  102 us
    all_to_all x1, blocking collectives, copy_for_each(): lax.all_to_all(jnp.broadcast_to(value[None], (size, *value.shape)), axis,...  60.2 us
    all_to_all x1, waiting for transfers between devices, copy_for_each(): lax.all_to_all(jnp.broadcast_to(value[None], (size, *value.shape)), axis,...  16.7 us
    all_to_all x1, starting transfers between devices, per_device(): lax.all_to_all(top[None], TP, split_axis=2, concat_axis=0, tiled=True)  7.48 us
    all_to_all x1, starting transfers between devices, copy_for_each(): lax.all_to_all(jnp.broadcast_to(value[None], (size, *value.shape)), axis,...  6.97 us
    all_to_all x1, waiting for transfers between devices, per_device(): lax.all_to_all(expanded[None], TP, split_axis=2, concat_axis=0, tiled=True)  6.34 us
    all_to_all x1, waiting for transfers between devices, per_device(): lax.all_to_all(total[None], TP, split_axis=2, concat_axis=0, tiled=True)  6.23 us
  transfers between devices with their start and end apart: 4, of which 4 were waited for; matrix products, arithmetic and copies ran while one was open for 1% of the time, Pallas kernels for 0%

commit v1 on v0

--- a/solution.py
+++ b/solution.py
@@ -15,7 +15,8 @@
 
 def over_axes(value, axes):
     for axis in axes:
-        value = lax.psum(value, axis)
+        blocks = lax.all_gather(value, axis)
+        value = jnp.sum(blocks, axis=0)
     return value
 
 

time: 242 us -> 317 us (1.31)
  blocking collectives: 162 us -> 237 us
  waiting for transfers between devices: 33 us -> 28.1 us
  starting transfers between devices: 23.7 us -> 27.3 us
  local copies, waits for them, and re-layouts: 5 us -> 8.32 us
    all_gather x0 -> x10, blocking collectives: none -> 138 us  [over_axes(): blocks = lax.all_gather(value, axis)]
    psum x6 -> x0, blocking collectives: 102 us -> none  [over_axes(): value = lax.psum(value, axis)]
    unnamed x0 -> x2, blocking collectives: none -> 38.9 us
    all_to_all x1, waiting for transfers between devices: 3.78 us -> 0.01 us  [per_device(): lax.all_to_all(top[None], TP, split_axis=2, concat_axis=0, tiled=True)]
  transfers between devices with their start and end apart: 4 -> 4, of which waited for: 4 -> 3; matrix products, arithmetic and copies ran while one was open for 1% -> 1% of each run, Pallas kernels for 0% -> 0%
where the time goes in v1:
time: 317 us
  blocking collectives  237 us (75%)
  waiting for transfers between devices  28.1 us (9%)
  starting transfers between devices  27.3 us (9%)
  other arithmetic  9.64 us (3%)
  local copies, waits for them, and re-layouts  8.32 us (3%)
  matrix products  4.03 us (1%)
    all_gather x10, blocking collectives, over_axes(): blocks = lax.all_gather(value, axis)  138 us
    all_to_all x1, blocking collectives, copy_for_each(): lax.all_to_all(jnp.broadcast_to(value[None], (size, *value.shape)), axis,...  60.2 us
    unnamed x2, blocking collectives  38.9 us
    all_to_all x1, waiting for transfers between devices, copy_for_each(): lax.all_to_all(jnp.broadcast_to(value[None], (size, *value.shape)), axis,...  15.6 us
    all_to_all x1, starting transfers between devices, copy_for_each(): lax.all_to_all(jnp.broadcast_to(value[None], (size, *value.shape)), axis,...  7.93 us
    all_to_all x1, starting transfers between devices, per_device(): lax.all_to_all(top[None], TP, split_axis=2, concat_axis=0, tiled=True)  7.48 us
    all_to_all x1, starting transfers between devices, per_device(): lax.all_to_all(total[None], TP, split_axis=2, concat_axis=0, tiled=True)  7.26 us
  transfers between devices with their start and end apart: 4, of which 3 were waited for; matrix products, arithmetic and copies ran while one was open for 1% of the time, Pallas kernels for 0%

profile of v1, /device:TPU:2, one launch (start us, length us, event | category | flops | bytes accessed | tf_op | source)
XLA Modules:
  0.0 316.8 jit_solution(11516388961491654941)
XLA Ops:
  0.7 1.4 dynamic-slice.5
  2.1 1.3 dynamic-slice.4
  4.7 0.7 convert_element_type.73
  5.3 0.7 convert_element_type.80
  6.0 0.8 fusion.36
  6.8 0.2 dynamic-update-slice
  7.0 36.5 %all-reduce.2 = f32[256]{0:T(256)S(1)} all-reduce(f32[256]{0:T(256)S(1)} %dynamic-update-slice), channel_id=2, replica_groups=mesh['kv_0'=16,'kv_1'=2,'tp_0'=4,'tp_1'=4] {'kv_0'}, use_global_device_ids=true, to_apply=%add.2 | all-reduce | flops 256 | bytes 2048
  43.5 0.7 broadcast_compare_fusion
  44.2 0.7 convert_element_type.75
  45.0 0.2 dynamic-update-slice.1
  45.3 2.4 all-reduce.3
  47.8 1.0 fusion.59
  48.9 29.3 %all-gather.2 = f32[256,512]{1,0:T(8,128)S(1)} all-gather(f32[16,512]{1,0:T(8,128)S(1)} %fusion.59), channel_id=4, replica_groups=mesh['kv_0'=16,'kv_1'=2,'tp_0'=4,'tp_1'=4] {'kv_0'}, dimensions={0}, use_global_device_ids=true | all-gather | bytes 557056 | tf_op jit(solution)/shard_map/all_gather | solution.py:18
  78.2 1.9 all-gather.3
  80.4 0.5 fusion.78
  80.9 0.7 convolution_convert_fusion
  82.1 0.4 fusion.85
  82.5 0.7 copy.58
  83.2 7.5 %all-to-all-start.1 = ((f32[1,16,16]{1,0,2:T(1,128)}), f32[1,16,16]{1,0,2:T(1,128)S(1)}, u32[]{:S(2)}, u32[]{:S(2)}) async-start(f32[1,16,16]{1,0,2:T(1,128)} %copy.58), calls=%async_computation.1 | async-start | bytes 16384 | tf_op jit(solution)/shard_map/all_to_all | solution.py:189
  90.7 0.2 fusion.9
  90.9 0.3 fusion.11
  91.4 28.0 %all-gather.6 = f32[256,32]{1,0:T(8,128)S(1)} all-gather(f32[16,32]{1,0:T(8,128)S(1)} %fusion.55), channel_id=8, replica_groups=mesh['kv_0'=16,'kv_1'=2,'tp_0'=4,'tp_1'=4] {'kv_0'}, dimensions={0}, use_global_device_ids=true | all-gather | bytes 34816 | tf_op jit(solution)/shard_map/all_gather | solution.py:18
  119.5 1.8 all-gather.7
  121.5 28.0 %all-gather.4 = f32[256,256]{1,0:T(8,128)S(1)} all-gather(f32[16,256]{1,0:T(8,128)S(1)} %fusion.57), channel_id=6, replica_groups=mesh['kv_0'=16,'kv_1'=2,'tp_0'=4,'tp_1'=4] {'kv_0'}, dimensions={0}, use_global_device_ids=true | all-gather | bytes 278528 | tf_op jit(solution)/shard_map/all_gather | solution.py:18
  149.5 0.2 fusion.86
  149.7 0.8 fusion.45
  150.5 0.7 reshape.436
  151.3 0.7 copy.59
  151.9 7.3 %all-to-all-start.2 = ((f32[1,16,16]{1,0,2:T(1,128)}), f32[1,16,16]{1,0,2:T(1,128)S(1)}, u32[]{:S(2)}, u32[]{:S(2)}) async-start(f32[1,16,16]{1,0,2:T(1,128)} %copy.59), calls=%async_computation.2 | async-start | bytes 16384 | tf_op jit(solution)/shard_map/all_to_all | solution.py:190
  159.2 6.2 %all-to-all-done.2 = f32[1,16,16]{1,0,2:T(1,128)S(1)} async-done(((f32[1,16,16]{1,0,2:T(1,128)}), f32[1,16,16]{1,0,2:T(1,128)S(1)}, u32[]{:S(2)}, u32[]{:S(2)}) %all-to-all-start.2) | async-done | bytes 1056 | tf_op jit(solution)/shard_map/all_to_all | solution.py:190
  165.4 4.6 %all-to-all-start = ((f32[16,1,1024]{2,1,0:T(1,128)}), f32[16,1,1024]{2,1,0:T(1,128)S(1)}, u32[]{:S(2)}, u32[]{:S(2)}) async-start(f32[16,1,1024]{2,1,0:T(1,128)} %reshape.436), calls=%async_computation | async-start | bytes 131072 | tf_op jit(solution)/shard_map/all_to_all | solution.py:191
  170.0 6.3 %all-to-all-done = f32[16,1,1024]{2,1,0:T(1,128)S(1)} async-done(((f32[16,1,1024]{2,1,0:T(1,128)}), f32[16,1,1024]{2,1,0:T(1,128)S(1)}, u32[]{:S(2)}, u32[]{:S(2)}) %all-to-all-start) | async-done | bytes 65568 | tf_op jit(solution)/shard_map/all_to_all | solution.py:191
  176.4 0.5 broadcast.257
  176.9 0.8 reduce.11
  177.9 0.8 reshape.438
  178.8 7.9 %all-to-all-start.3 = ((f32[32,1,1152]{2,1,0:T(1,128)}), f32[32,1,1152]{2,1,0:T(1,128)S(1)}, u32[]{:S(2)}, u32[]{:S(2)}) async-start(f32[32,1,1152]{2,1,0:T(1,128)} %reshape.438), calls=%async_computation.3 | async-start | bytes 294912 | tf_op jit(solution)/shard_map/all_to_all | solution.py:25
  186.8 1.8 all-gather.5
  189.0 15.6 %all-to-all-done.3 = f32[32,1,1152]{2,1,0:T(1,128)S(1)} async-done(((f32[32,1,1152]{2,1,0:T(1,128)}), f32[32,1,1152]{2,1,0:T(1,128)S(1)}, u32[]{:S(2)}, u32[]{:S(2)}) %all-to-all-start.3) | async-done | bytes 147488 | tf_op jit(solution)/shard_map/all_to_all | solution.py:25
  204.6 1.0 reduce.12
  206.7 0.3 fusion.5
  207.0 11.9 %all-gather.8 = f32[64,64]{1,0:T(8,128)S(1)} all-gather(f32[16,64]{1,0:T(8,128)S(1)} %fusion.5), channel_id=10, replica_groups=mesh['kv_0'=16,'kv_1'=2,'tp_0'=4,'tp_1'=4] {'tp_0'}, dimensions={0}, use_global_device_ids=true | all-gather | bytes 20480 | tf_op jit(solution)/shard_map/all_gather | solution.py:18
  218.9 11.3 %all-gather.9 = f32[64,64]{1,0:T(8,128)S(1)} all-gather(f32[16,64]{1,0:T(8,128)S(1)} %reduce_sum.197), channel_id=11, replica_groups=mesh['kv_0'=16,'kv_1'=2,'tp_0'=4,'tp_1'=4] {'tp_1'}, dimensions={0}, use_global_device_ids=true | all-gather | bytes 20480 | tf_op jit(solution)/shard_map/all_gather | solution.py:18
  230.5 0.5 broadcast_in_dim.35
  231.1 60.2 %all_to_all.68 = f32[32,1,8208]{2,1,0:T(1,128)S(1)} all-to-all(f32[32,1,8208]{2,1,0:T(1,128)S(1)} %broadcast_in_dim.35), channel_id=1, replica_groups=mesh['kv_0'=16,'kv_1'=2,'tp_0'=4,'tp_1'=4] {'kv_0','kv_1'}, dimensions={0} | all-to-all | bytes 2101248 | tf_op jit(solution)/shard_map/all_to_all | solution.py:25
  291.3 0.6 reduce_sum.200
  292.3 11.9 %all-gather.10 = f32[64,64]{1,0:T(8,128)S(1)} all-gather(f32[16,64]{1,0:T(8,128)S(1)} %fusion.23), channel_id=12, replica_groups=mesh['kv_0'=16,'kv_1'=2,'tp_0'=4,'tp_1'=4] {'tp_0'}, dimensions={0}, use_global_device_ids=true | all-gather | bytes 20480 | tf_op jit(solution)/shard_map/all_gather | solution.py:18
  304.2 11.9 %all-gather.11 = f32[64,64]{1,0:T(8,128)S(1)} all-gather(f32[16,64]{1,0:T(8,128)S(1)} %reduce_sum.201), channel_id=13, replica_groups=mesh['kv_0'=16,'kv_1'=2,'tp_0'=4,'tp_1'=4] {'tp_1'}, dimensions={0}, use_global_device_ids=true | all-gather | bytes 20480 | tf_op jit(solution)/shard_map/all_gather | solution.py:18
  316.2 0.6 add_convert_fusion.1
  (119 shorter events, 4.0 us)
Async XLA Ops:
  0.6 80.2 %copy-start = (bf16[512,16,64]{0,2,1:T(8,128)(2,1)S(1)}, bf16[512,16,64]{0,2,1:T(8,128)(2,1)}, u32[]{:S(2)}) copy-start(bf16[512,16,64]{0,2,1:T(8,128)(2,1)} %param.27) | copy-start | bytes 3145732
  0.6 79.7 %copy-start.3 = (bf16[512,16,32]{0,2,1:T(8,128)(2,1)S(1)}, bf16[512,16,32]{0,2,1:T(8,128)(2,1)}, u32[]{:S(2)}) copy-start(bf16[512,16,32]{0,2,1:T(8,128)(2,1)} %param.28) | copy-start | bytes 1572868
  47.8 33.0 %copy-start.4 = (bf16[256,16,64]{0,2,1:T(8,128)(2,1)S(1)}, bf16[256,16,64]{0,2,1:T(8,128)(2,1)}, u32[]{:S(2)}) copy-start(bf16[256,16,64]{0,2,1:T(8,128)(2,1)} %param.30) | copy-start | bytes 1572868
  80.9 0.9 copy-start.6
  80.9 1.2 copy-start.1
  82.1 9.0 %copy-start.5 = (bf16[16,64]{1,0:T(8,128)(2,1)S(1)}, bf16[16,64]{1,0:T(8,128)(2,1)}, u32[]{:S(2)}) copy-start(bf16[16,64]{1,0:T(8,128)(2,1)} %param.18) | copy-start | bytes 6148
  82.1 9.0 %copy-start.9 = (bf16[64,32]{0,1:T(8,128)(2,1)S(1)}, bf16[64,32]{0,1:T(8,128)(2,1)}, u32[]{:S(2)}) copy-start(bf16[64,32]{0,1:T(8,128)(2,1)} %param.25) | copy-start | bytes 12292
  82.1 9.2 %copy-start.8 = (bf16[64,256]{1,0:T(8,128)(2,1)S(1)}, bf16[64,256]{1,0:T(8,128)(2,1)}, u32[]{:S(2)}) copy-start(bf16[64,256]{1,0:T(8,128)(2,1)} %param.24) | copy-start | bytes 98308
  82.5 67.0 %copy-start.2 = (bf16[256,16,64]{0,2,1:T(8,128)(2,1)S(1)}, bf16[256,16,64]{0,2,1:T(8,128)(2,1)}, u32[]{:S(2)}) copy-start(bf16[256,16,64]{0,2,1:T(8,128)(2,1)} %param.31) | copy-start | bytes 1572868
  83.2 68.7 %all-to-all-start.1 = ((f32[1,16,16]{1,0,2:T(1,128)}), f32[1,16,16]{1,0,2:T(1,128)S(1)}, u32[]{:S(2)}, u32[]{:S(2)}) async-start(f32[1,16,16]{1,0,2:T(1,128)} %copy.58), calls=%async_computation.1 | async-start | bytes 16384 | tf_op jit(solution)/shard_map/all_to_all | solution.py:189
  150.5 36.2 %copy-start.13 = (bf16[64]{0:T(256)(128)(2,1)S(1)}, bf16[64]{0:T(256)(128)(2,1)}, u32[]{:S(2)}) copy-start(bf16[64]{0:T(256)(128)(2,1)} %param.33) | copy-start | bytes 388
  150.5 36.2 %copy-start.14 = (bf16[256]{0:T(256)(128)(2,1)S(1)}, bf16[256]{0:T(256)(128)(2,1)}, u32[]{:S(2)}) copy-start(bf16[256]{0:T(256)(128)(2,1)} %param.29) | copy-start | bytes 1540
  151.9 13.5 %all-to-all-start.2 = ((f32[1,16,16]{1,0,2:T(1,128)}), f32[1,16,16]{1,0,2:T(1,128)S(1)}, u32[]{:S(2)}, u32[]{:S(2)}) async-start(f32[1,16,16]{1,0,2:T(1,128)} %copy.59), calls=%async_computation.2 | async-start | bytes 16384 | tf_op jit(solution)/shard_map/all_to_all | solution.py:190
  165.4 11.0 %all-to-all-start = ((f32[16,1,1024]{2,1,0:T(1,128)}), f32[16,1,1024]{2,1,0:T(1,128)S(1)}, u32[]{:S(2)}, u32[]{:S(2)}) async-start(f32[16,1,1024]{2,1,0:T(1,128)} %reshape.436), calls=%async_computation | async-start | bytes 131072 | tf_op jit(solution)/shard_map/all_to_all | solution.py:191
  178.8 25.8 %all-to-all-start.3 = ((f32[32,1,1152]{2,1,0:T(1,128)}), f32[32,1,1152]{2,1,0:T(1,128)S(1)}, u32[]{:S(2)}, u32[]{:S(2)}) async-start(f32[32,1,1152]{2,1,0:T(1,128)} %reshape.438), calls=%async_computation.3 | async-start | bytes 294912 | tf_op jit(solution)/shard_map/all_to_all | solution.py:25
  189.0 17.7 %copy-start.10 = (bf16[16,256]{1,0:T(8,128)(2,1)}, bf16[16,256]{1,0:T(8,128)(2,1)S(1)}, u32[]{:S(2)}) copy-start(bf16[16,256]{1,0:T(8,128)(2,1)S(1)} %get-tuple-element.20) | copy-start | bytes 24580
  205.6 1.1 copy-start.12
  205.8 24.6 %copy-start.7 = (bf16[64,512]{1,0:T(8,128)(2,1)S(1)}, bf16[64,512]{1,0:T(8,128)(2,1)}, u32[]{:S(2)}) copy-start(bf16[64,512]{1,0:T(8,128)(2,1)} %param.34) | copy-start | bytes 196612
  291.3 0.8 copy-start.11
